TPU v7x, 32 devices: a whole 2x2x4 slice. The times are simulated.
32 devices in a mesh: grp: 2 (over y), fs: 4 (over z), tp: 4 (over x, core).
Axes of the slice: x: 2, y: 2, z: 4, core: 2. Of those that a mesh axis runs over, the one named last changes fastest.
Arguments:
- tokens: bfloat16 [4096, 2048], P(('grp', 'fs', 'tp')), parts along dimension 0, may hold values from -6 to 6
- up_master: float32 [2048, 4096], P('fs', 'tp'), may hold values from -0.125 to 0.125
- down_master: float32 [4096, 2048], P('fs', 'tp'), may hold values from -0.09375 to 0.09375
- norm_gain: float32 [2048], P('fs'), may hold values from 0.1 to 1.9
Outputs:
- up_weights: bfloat16 [4096, 4096], P('grp', 'tp'), parts along dimension 0
- down_weights: bfloat16 [8192, 2048], P(('grp', 'tp')), parts along dimension 0
- mlp_output: bfloat16 [4096, 2048], P(('grp', 'fs', 'tp')), parts along dimension 0
There are 2 independent parts, one for each index of `grp`. A program takes and returns all parts, laid end to end along the dimension named above; an argument that names none is the same for every part. Nothing has to cross between parts.
All inputs are finite; a program needn't handle non-finite values.
Results may differ from a plain program's by a relative error of at most 0.014.
Values may be sent and summed in bfloat16 or wider, within the bound.
A program may use at most 64 MiB of HBM per device.

v0:
```python
import jax
import jax.numpy as jnp
from jax import lax
from jax.sharding import PartitionSpec as P


def on_device(tokens, up_master, down_master, norm_gain):
    up_local = (norm_gain[:, None] * up_master).astype(jnp.bfloat16)
    down_local = down_master.astype(jnp.bfloat16)
    float_tokens = tokens.astype(jnp.float32)
    scale = lax.rsqrt(jnp.mean(float_tokens * float_tokens, axis=-1, keepdims=True) + 1e-06)
    normed_local = (float_tokens * scale).astype(jnp.bfloat16)
    normed = lax.all_gather(normed_local, "tp", axis=0, tiled=True)
    up_weights = lax.all_gather(up_local, "fs", axis=0, tiled=True)
    preact = jnp.dot(normed, up_weights, preferred_element_type=jnp.float32)
    gathered_rows = lax.all_gather(down_local, "fs", axis=0, tiled=True)
    down_weights = lax.all_to_all(gathered_rows, "tp", split_axis=0, concat_axis=1, tiled=True)
    rectified = jax.nn.relu(preact)
    hidden = (rectified * rectified).astype(jnp.bfloat16)
    mlp_output = lax.psum_scatter(
        jnp.dot(hidden, down_weights, preferred_element_type=jnp.float32).astype(jnp.bfloat16),
        "tp",
        scatter_dimension=0,
        tiled=True,
    )
    return (up_weights, down_weights, mlp_output)


def solution(mesh):
    in_specs = (P(("grp", "fs", "tp"), None), P("fs", "tp"), P("fs", "tp"), P("fs"))
    out_specs = (P("grp", "tp"), P(("grp", "tp"), None), P(("grp", "fs", "tp"), None))
    return jax.shard_map(
        on_device, mesh=mesh, in_specs=in_specs, out_specs=out_specs, check_vma=False
    )
```

profile of v0, /device:TPU:0, one launch (start us, length us, event | category | flops | bytes accessed | tf_op | source)
XLA Modules:
  0.0 262.0 jit_solution(9083774294734147993)
XLA Ops:
  7.2 0.0 copy-start.1
  7.2 0.0 all-gather.6.cloned.1.call-start
  7.2 2.7 %convert_element_type.19 = bf16[1024,512]{1,0:T(8,128)(2,1)} convert(f32[1024,512]{1,0:T(8,128)} %param.6) | non-fusion elementwise | flops 524288 | bytes 3145728 | tf_op jit(solution)/shard_map/convert_element_type | solution.py:9
  10.0 0.0 copy-start
  10.0 0.0 copy-start.2
  10.0 0.0 all-gather.6.cloned.1.call-update
  10.0 0.0 all-gather.8.cloned.1.call-start
  10.0 0.0 copy-done.1
  10.1 0.2 fusion
  10.2 1.0 fusion.1
  11.2 0.0 all-gather.8.cloned.1.call-update
  11.2 0.0 all-gather.4.cloned.1.call-start
  11.3 0.5 copy-done
  11.7 0.0 copy-done.2
  11.7 1.1 multiply_convert_fusion.1
  12.9 0.0 all-gather.4.cloned.1.call-update
  12.9 0.0 reduce-scatter.2.cloned.1.call-start
  13.0 80.7 %all-gather.6.cloned.1.call-done = bf16[4096,512]{1,0:T(8,128)(2,1)} async-done(((bf16[1024,512]{1,0:T(8,128)(2,1)}), bf16[4096,512]{1,0:T(8,128)(2,1)}) %all-gather.6.cloned.1.call-update) | async-done | bytes 4194320 | tf_op jit(solution)/shard_map/all_gather | solution.py:16
  93.6 65.1 %all_to_all.19 = bf16[4,1024,512]{2,1,0:T(8,128)(2,1)} all-to-all(bf16[4,1024,512]{2,1,0:T(8,128)(2,1)} %bitcast.9), channel_id=1, replica_groups=mesh['grp'=2,'fs'=4,'tp'=4] {'tp'}, dimensions={0} | all-to-all | bytes 8388608 | tf_op jit(solution)/shard_map/all_to_all | solution.py:17
  158.7 6.2 %copy.8 = bf16[4,1024,512]{1,2,0:T(8,128)(2,1)} copy(bf16[4,1024,512]{2,1,0:T(8,128)(2,1)} %all_to_all.19) | data formatting | bytes 8388608 | tf_op jit(solution)/shard_map/all_to_all | solution.py:17
  164.9 0.0 all-gather.8.cloned.1.call-done
  164.9 46.2 %all-gather.4.cloned.1.call-done = bf16[2048,1024]{1,0:T(8,128)(2,1)} async-done(((bf16[512,1024]{1,0:T(8,128)(2,1)}), bf16[2048,1024]{1,0:T(8,128)(2,1)}) %all-gather.4.cloned.1.call-update) | async-done | bytes 4194320 | tf_op jit(solution)/shard_map/all_gather | solution.py:14
  211.1 9.9 %convolution_convert_fusion = bf16[512,2048]{1,0:T(8,128)(2,1)} fusion(bf16[1024,2048]{0,1:T(8,128)(2,1)} %bitcast.7, bf16[512,2048]{1,0:T(8,128)(2,1)} %all-gather.8.cloned.1.call-done, bf16[2048,1024]{1,0:T(8,128)(2,1)} %all-gather.4.cloned.1.call-done), kind=kOutput, calls=%fused_computation | convolution fusion | flops 4297588736 | bytes 12582912 | tf_op jit(solution)/shard_map/dot_general | solution.py:21
  221.0 0.0 reduce-scatter.2.cloned.1.call-update
  221.0 6.4 %copy.9 = bf16[1024,2048]{1,0:T(8,128)(2,1)} copy(bf16[1024,2048]{0,1:T(8,128)(2,1)} %bitcast.8) | data formatting | bytes 8388608
  227.4 23.4 %reduce-scatter.2.cloned.1.call-done = bf16[128,2048]{1,0:T(8,128)(2,1)} async-done(((bf16[512,2048]{1,0:T(8,128)(2,1)}), bf16[128,2048]{1,0:T(8,128)(2,1)}) %reduce-scatter.2.cloned.1.call-update) | async-done | bytes 524304 | tf_op jit(solution)/shard_map/reduce_scatter | solution.py:20
  250.8 4.6 %copy.11 = bf16[2048,1024]{1,0:T(8,128)(2,1)} copy(bf16[2048,1024]{1,0:T(8,128)(2,1)} %all-gather.4.cloned.1.call-done) | data formatting | bytes 8388608
  (1 shorter events, 0.0 us)
Async XLA Ops:
  7.2 2.9 %copy-start.1 = (bf16[128,2048]{1,0:T(8,128)(2,1)S(1)}, bf16[128,2048]{1,0:T(8,128)(2,1)}, u32[]{:S(2)}) copy-start(bf16[128,2048]{1,0:T(8,128)(2,1)} %param.4) | copy-start | bytes 1572868
  7.2 86.4 %all-gather.6.cloned.1.call-start = ((), (), s32[]{:S(2)}) async-start(), calls=%async_computation.3 | async-start | bytes 5242880 | tf_op jit(solution)/shard_map/all_gather | solution.py:16
  10.0 1.8 copy-start
  10.0 1.8 copy-start.2
  10.0 154.9 %all-gather.8.cloned.1.call-start = ((), (), s32[]{:S(2)}) async-start(), calls=%async_computation.4 | async-start | bytes 2621440 | tf_op jit(solution)/shard_map/all_gather | solution.py:13
  11.2 199.9 %all-gather.4.cloned.1.call-start = ((), (), s32[]{:S(2)}) async-start(), calls=%async_computation.2 | async-start | bytes 5242880 | tf_op jit(solution)/shard_map/all_gather | solution.py:14
  12.9 237.9 %reduce-scatter.2.cloned.1.call-start = ((), (), s32[]{:S(2)}) async-start(), calls=%async_computation.5 | async-start | bytes 2621440 | tf_op jit(solution)/shard_map/reduce_scatter | solution.py:20
Sparse Core Ops, SparseCore 0:
  10.1 83.4 all-gather.5
  95.8 32.3 all-gather.7
  130.3 80.7 all-gather.3
  221.1 29.6 reduce-scatter.1
where the time goes:
time: 263 us; the launch traced here: 262 us
  waiting for transfers between devices  150 us (57%)
  blocking collectives  65.1 us (25%)
  local copies, waits for them, and re-layouts  17.8 us (7%)
  between operations  13.8 us (5%)
  matrix products  9.89 us (4%)
  other arithmetic  5.04 us (2%)
    all_gather x1, waiting for transfers between devices, on_device(): gathered_rows = lax.all_gather(down_local, 'fs', axis=0, tiled=True)  80.7 us
    all_to_all x1, blocking collectives, on_device(): lax.all_to_all(gathered_rows, 'tp', split_axis=0, concat_axis=1, tiled=True)  65.1 us
    all_gather x1, waiting for transfers between devices, on_device(): up_weights = lax.all_gather(up_local, 'fs', axis=0, tiled=True)  46.2 us
    reduce_scatter x1, waiting for transfers between devices, on_device(): lax.psum_scatter(jnp.dot(hidden, down_weights, preferred_element_type=jnp...  23.4 us
    unnamed x8, local copies, waits for them, and re-layouts  11.5 us
    dot_general x1, matrix products, on_device(): jnp.dot(hidden, down_weights, preferred_element_type=jnp.float32)  9.89 us
    all_to_all x1, local copies, waits for them, and re-layouts, on_device(): lax.all_to_all(gathered_rows, 'tp', split_axis=0, concat_axis=1, tiled=True)  6.21 us
  transfers between devices with their start and end apart: 4, of which 3 were waited for; matrix products, arithmetic and copies ran while one was open for 6% of the time, Pallas kernels for 0%

commit v1 on v0

--- a/solution.py
+++ b/solution.py
@@ -2,6 +2,20 @@
 import jax.numpy as jnp
 from jax import lax
 from jax.sharding import PartitionSpec as P
+
+
+def stages_all_post(block_in):
+    mesh_name = "fs"
+    size_here = lax.axis_size(mesh_name)
+    mat_out = [(idx - 1, idx) for idx in range(1, size_here)] + [(size_here - 1, 0)]
+    inter = block_in
+    ledger = [inter]
+    for _ in [*range(size_here - 1)]:
+        inter = lax.ppermute(inter, mesh_name, mat_out)
+        ledger += [inter]
+    v1 = jnp.concatenate([*reversed(ledger)], 0)
+    arr_now = lax.axis_index(mesh_name)
+    return jnp.roll(v1, (arr_now + 1) * inter.shape[0], axis=0)
 
 
 def on_device(tokens, up_master, down_master, norm_gain):
@@ -11,7 +25,7 @@
     scale = lax.rsqrt(jnp.mean(float_tokens * float_tokens, axis=-1, keepdims=True) + 1e-06)
     normed_local = (float_tokens * scale).astype(jnp.bfloat16)
     normed = lax.all_gather(normed_local, "tp", axis=0, tiled=True)
-    up_weights = lax.all_gather(up_local, "fs", axis=0, tiled=True)
+    up_weights = stages_all_post(up_local)
     preact = jnp.dot(normed, up_weights, preferred_element_type=jnp.float32)
     gathered_rows = lax.all_gather(down_local, "fs", axis=0, tiled=True)
     down_weights = lax.all_to_all(gathered_rows, "tp", split_axis=0, concat_axis=1, tiled=True)

time: 263 us -> 247 us (0.939)
  blocking collectives: 65.1 us -> 0 us
  starting transfers between devices: 0.16 us -> 22.5 us
  waiting for transfers between devices: 150 us -> 171 us
  local copies, waits for them, and re-layouts: 17.8 us -> 20.7 us
    ppermute x0 -> x3, waiting for transfers between devices: none -> 66.4 us  [stages_all_post(): inter = lax.ppermute(inter, mesh_name, mat_out)]
    all_to_all x1 -> x0, blocking collectives: 65.1 us -> none  [on_device(): lax.all_to_all(gathered_rows, 'tp', split_axis=0, concat_axis=1, tiled=True)]
    all_gather x1 -> x0, waiting for transfers between devices: 46.2 us -> none  [on_device(): up_weights = lax.all_gather(up_local, 'fs', axis=0, tiled=True)]
    all_to_all x0 -> x1, waiting for transfers between devices: none -> 21.5 us  [on_device(): lax.all_to_all(gathered_rows, 'tp', split_axis=0, concat_axis=1, tiled=True)]
    all_gather x1, waiting for transfers between devices: 80.7 us -> 61.1 us  [on_device(): gathered_rows = lax.all_gather(down_local, 'fs', axis=0, tiled=True)]
    ppermute x0 -> x3, starting transfers between devices: none -> 17.5 us  [stages_all_post(): inter = lax.ppermute(inter, mesh_name, mat_out)]
    all_to_all x0 -> x1, starting transfers between devices: none -> 4.84 us  [on_device(): lax.all_to_all(gathered_rows, 'tp', split_axis=0, concat_axis=1, tiled=True)]
    unnamed x8 -> x11, local copies, waits for them, and re-layouts: 11.5 us -> 11.9 us
  transfers between devices with their start and end apart: 4 -> 7, of which waited for: 3 -> 5; matrix products, arithmetic and copies ran while one was open for 6% -> 10% of each run, Pallas kernels for 0% -> 0%
where the time goes in v1:
time: 247 us; the launch traced here: 246 us
  waiting for transfers between devices  171 us (69%)
  starting transfers between devices  22.5 us (9%)
  local copies, waits for them, and re-layouts  20.7 us (8%)
  between operations  15.6 us (6%)
  matrix products  9.9 us (4%)
  other arithmetic  6.58 us (3%)
    ppermute x3, waiting for transfers between devices, stages_all_post(): inter = lax.ppermute(inter, mesh_name, mat_out)  66.4 us
    all_gather x1, waiting for transfers between devices, on_device(): gathered_rows = lax.all_gather(down_local, 'fs', axis=0, tiled=True)  61.1 us
    reduce_scatter x1, waiting for transfers between devices, on_device(): lax.psum_scatter(jnp.dot(hidden, down_weights, preferred_element_type=jnp...  22.1 us
    all_to_all x1, waiting for transfers between devices, on_device(): lax.all_to_all(gathered_rows, 'tp', split_axis=0, concat_axis=1, tiled=True)  21.5 us
    ppermute x3, starting transfers between devices, stages_all_post(): inter = lax.ppermute(inter, mesh_name, mat_out)  17.5 us
    unnamed x11, local copies, waits for them, and re-layouts  11.9 us
    dot_general x1, matrix products, on_device(): jnp.dot(hidden, down_weights, preferred_element_type=jnp.float32)  9.9 us
    all_to_all x1, local copies, waits for them, and re-layouts, on_device(): lax.all_to_all(gathered_rows, 'tp', split_axis=0, concat_axis=1, tiled=True)  6.31 us
  transfers between devices with their start and end apart: 7, of which 5 were waited for; matrix products, arithmetic and copies ran while one was open for 10% of the time, Pallas kernels for 0%

profile of v1, /device:TPU:0, one launch (start us, length us, event | category | flops | bytes accessed | tf_op | source)
XLA Modules:
  0.0 246.4 jit_solution(6121737993728472597)
XLA Ops:
  8.0 0.0 all-gather.3.cloned.1.call-start
  8.1 2.8 %convert_element_type.19 = bf16[1024,512]{1,0:T(8,128)(2,1)} convert(f32[1024,512]{1,0:T(8,128)} %param.6) | non-fusion elementwise | flops 524288 | bytes 3145728 | tf_op jit(solution)/shard_map/convert_element_type | solution.py:23
  10.9 0.0 all-gather.3.cloned.1.call-update
  10.9 0.2 multiply_convert_fusion.1
  11.1 3.1 %collective-permute-start = (bf16[512,1024]{1,0:T(8,128)(2,1)S(1)}, bf16[512,1024]{1,0:T(8,128)(2,1)S(1)}, u32[]{:S(2)}, u32[]{:S(2)}) collective-permute-start(bf16[512,1024]{1,0:T(8,128)(2,1)S(1)} %multiply_convert_fusion.1), channel_id=1, source_target_pairs={{0,4},{4,8},{8,12},{12,0},{1,5},{5,9},{9,13},{13,1},{2,6},{6,10},{... | collective-permute-start | bytes 3145736 | tf_op jit(solution)/shard_map/ppermute | solution.py:14
  14.2 38.9 %collective-permute-done = bf16[512,1024]{1,0:T(8,128)(2,1)S(1)} collective-permute-done((bf16[512,1024]{1,0:T(8,128)(2,1)S(1)}, bf16[512,1024]{1,0:T(8,128)(2,1)S(1)}, u32[]{:S(2)}, u32[]{:S(2)}) %collective-permute-start) | collective-permute-done | bytes 1048608 | tf_op jit(solution)/shard_map/ppermute | solution.py:14
  53.1 14.3 %collective-permute-start.1 = (bf16[512,1024]{1,0:T(8,128)(2,1)S(1)}, bf16[512,1024]{1,0:T(8,128)(2,1)}, u32[]{:S(2)}, u32[]{:S(2)}) collective-permute-start(bf16[512,1024]{1,0:T(8,128)(2,1)S(1)} %collective-permute-done), channel_id=1, source_target_pairs={{0,4},{4,8},{8,12},{12,0},{1,5},{5,9},{9,13},{13,1},{2,6},{6,10},{... | collective-permute-start | bytes 3145736 | tf_op jit(solution)/shard_map/ppermute | solution.py:14
  67.4 1.2 fusion
  68.7 61.1 %all-gather.3.cloned.1.call-done = bf16[4096,512]{1,0:T(8,128)(2,1)} async-done(((bf16[1024,512]{1,0:T(8,128)(2,1)}), bf16[4096,512]{1,0:T(8,128)(2,1)}) %all-gather.3.cloned.1.call-update) | async-done | bytes 4194320 | tf_op jit(solution)/shard_map/all_gather | solution.py:30
  129.8 4.8 %all-to-all-start = ((bf16[4,1024,512]{2,1,0:T(8,128)(2,1)}), bf16[4,1024,512]{2,1,0:T(8,128)(2,1)}, u32[]{:S(2)}, u32[]{:S(2)}) async-start(bf16[4,1024,512]{2,1,0:T(8,128)(2,1)} %bitcast.9), calls=%async_computation | async-start | bytes 8388608 | tf_op jit(solution)/shard_map/all_to_all | solution.py:31
  134.7 0.0 all-gather.5.cloned.1.call-start
  134.7 2.0 fusion.1
  136.7 0.0 all-gather.5.cloned.1.call-update
  136.7 0.0 reduce-scatter.2.cloned.1.call-start
  136.8 0.0 collective-permute-done.1
  136.8 0.1 collective-permute-start.2
  136.9 27.6 %collective-permute-done.2 = bf16[512,1024]{1,0:T(8,128)(2,1)} collective-permute-done((bf16[512,1024]{1,0:T(8,128)(2,1)}, bf16[512,1024]{1,0:T(8,128)(2,1)}, u32[]{:S(2)}, u32[]{:S(2)}) %collective-permute-start.2) | collective-permute-done | bytes 1048608 | tf_op jit(solution)/shard_map/ppermute | solution.py:14
  164.4 1.3 constant_dynamic-update-slice_fusion.7
  165.7 1.3 constant_dynamic-update-slice_fusion.6
  167.0 0.1 constant_dynamic-update-slice_fusion.5
  167.1 0.2 constant_dynamic-update-slice_fusion.4
  167.3 1.3 constant_dynamic-update-slice_fusion.3
  168.6 1.3 constant_dynamic-update-slice_fusion.2
  169.9 0.1 constant_dynamic-update-slice_fusion.1
  170.0 0.2 constant_dynamic-update-slice_fusion
  170.2 2.5 constant_dynamic-slice_fusion
  172.6 21.5 %all-to-all-done = bf16[4,1024,512]{2,1,0:T(8,128)(2,1)} async-done(((bf16[4,1024,512]{2,1,0:T(8,128)(2,1)}), bf16[4,1024,512]{2,1,0:T(8,128)(2,1)}, u32[]{:S(2)}, u32[]{:S(2)}) %all-to-all-start) | async-done | bytes 4194336 | tf_op jit(solution)/shard_map/all_to_all | solution.py:31
  194.1 6.3 %copy.8 = bf16[4,1024,512]{1,2,0:T(8,128)(2,1)} copy(bf16[4,1024,512]{2,1,0:T(8,128)(2,1)} %all-to-all-done) | data formatting | bytes 8388608 | tf_op jit(solution)/shard_map/all_to_all | solution.py:31
  200.4 9.9 %convolution_convert_fusion = bf16[512,2048]{1,0:T(8,128)(2,1)} fusion(bf16[1024,2048]{0,1:T(8,128)(2,1)} %bitcast.7, bf16[512,2048]{1,0:T(8,128)(2,1)} %all-gather.5.cloned.1.call-done, bf16[2048,1024]{1,0:T(8,128)(2,1)} %constant_dynamic-slice_fusion), kind=kOutput, calls=%fused_computation | convolution fusion | flops 4297588736 | bytes 12582912 | tf_op jit(solution)/shard_map/dot_general | solution.py:35
  210.3 0.0 reduce-scatter.2.cloned.1.call-update
  210.3 6.5 %copy.9 = bf16[1024,2048]{1,0:T(8,128)(2,1)} copy(bf16[1024,2048]{0,1:T(8,128)(2,1)} %bitcast.8) | data formatting | bytes 8388608
  216.9 22.1 %reduce-scatter.2.cloned.1.call-done = bf16[128,2048]{1,0:T(8,128)(2,1)} async-done(((bf16[512,2048]{1,0:T(8,128)(2,1)}), bf16[128,2048]{1,0:T(8,128)(2,1)}) %reduce-scatter.2.cloned.1.call-update) | async-done | bytes 524304 | tf_op jit(solution)/shard_map/reduce_scatter | solution.py:34
  (6 shorter events, 0.0 us)
Async XLA Ops:
  8.0 2.9 %copy-start = (f32[512,1024]{1,0:T(8,128)S(1)}, f32[512,1024]{1,0:T(8,128)}, u32[]{:S(2)}) copy-start(f32[512,1024]{1,0:T(8,128)} %param.5) | copy-start | bytes 6291460
  8.0 2.9 %copy-start.1 = (f32[512]{0:T(512)S(1)}, f32[512]{0:T(512)}, u32[]{:S(2)}) copy-start(f32[512]{0:T(512)} %param.7) | copy-start | bytes 6148
  8.0 121.8 %all-gather.3.cloned.1.call-start = ((), (), s32[]{:S(2)}) async-start(), calls=%async_computation.2 | async-start | bytes 5242880 | tf_op jit(solution)/shard_map/all_gather | solution.py:30
  11.1 42.0 %collective-permute-start = (bf16[512,1024]{1,0:T(8,128)(2,1)S(1)}, bf16[512,1024]{1,0:T(8,128)(2,1)S(1)}, u32[]{:S(2)}, u32[]{:S(2)}) collective-permute-start(bf16[512,1024]{1,0:T(8,128)(2,1)S(1)} %multiply_convert_fusion.1), channel_id=1, source_target_pairs={{0,4},{4,8},{8,12},{12,0},{1,5},{5,9},{9,13},{13,1},{2,6},{6,10},{... | collective-permute-start | bytes 3145736 | tf_op jit(solution)/shard_map/ppermute | solution.py:14
  53.1 83.7 %collective-permute-start.1 = (bf16[512,1024]{1,0:T(8,128)(2,1)S(1)}, bf16[512,1024]{1,0:T(8,128)(2,1)}, u32[]{:S(2)}, u32[]{:S(2)}) collective-permute-start(bf16[512,1024]{1,0:T(8,128)(2,1)S(1)} %collective-permute-done), channel_id=1, source_target_pairs={{0,4},{4,8},{8,12},{12,0},{1,5},{5,9},{9,13},{13,1},{2,6},{6,10},{... | collective-permute-start | bytes 3145736 | tf_op jit(solution)/shard_map/ppermute | solution.py:14
  129.8 64.3 %all-to-all-start = ((bf16[4,1024,512]{2,1,0:T(8,128)(2,1)}), bf16[4,1024,512]{2,1,0:T(8,128)(2,1)}, u32[]{:S(2)}, u32[]{:S(2)}) async-start(bf16[4,1024,512]{2,1,0:T(8,128)(2,1)} %bitcast.9), calls=%async_computation | async-start | bytes 8388608 | tf_op jit(solution)/shard_map/all_to_all | solution.py:31
  134.7 65.8 %all-gather.5.cloned.1.call-start = ((), (), s32[]{:S(2)}) async-start(), calls=%async_computation.3 | async-start | bytes 2621440 | tf_op jit(solution)/shard_map/all_gather | solution.py:27
  136.7 102.2 %reduce-scatter.2.cloned.1.call-start = ((), (), s32[]{:S(2)}) async-start(), calls=%async_computation.4 | async-start | bytes 2621440 | tf_op jit(solution)/shard_map/reduce_scatter | solution.py:34
  136.8 27.6 %collective-permute-start.2 = (bf16[512,1024]{1,0:T(8,128)(2,1)}, bf16[512,1024]{1,0:T(8,128)(2,1)}, u32[]{:S(2)}, u32[]{:S(2)}) collective-permute-start(bf16[512,1024]{1,0:T(8,128)(2,1)} %collective-permute-done.1), channel_id=1, source_target_pairs={{0,4},{4,8},{8,12},{12,0},{1,5},{5,9},{9,13},{13,1},{2,6},{6,10},{... | collective-permute-start | bytes 3145736 | tf_op jit(solution)/shard_map/ppermute | solution.py:14
Sparse Core Ops, SparseCore 0:
  11.0 118.7 all-gather.2
Sparse Core Ops, SparseCore 1:
  137.3 32.6 all-gather.4
  210.4 28.5 reduce-scatter.1
